TPU v7x, 32 devices: a whole 2x2x4 slice. The times are simulated.
32 devices in a mesh: ep: 16 (over z, y, x), tp: 2 (over core).
Axes of the slice: x: 2, y: 2, z: 4, core: 2. Of those that a mesh axis runs over, the one named last changes fastest.
Arguments:
- hidden: bfloat16 [1024, 2048], P('ep'), may hold values from -6 to 6
- mix_gain: float32 [2048], replicated, may hold values from 0.1 to 1.9
- recept_weight: bfloat16 [2048, 1024], P(None, 'tp'), may hold values from -0.125 to 0.125
- key_weight: bfloat16 [2048, 1024], P(None, 'tp'), may hold values from -0.125 to 0.125
- value_weight: bfloat16 [2048, 1024], P(None, 'tp'), may hold values from -0.125 to 0.125
- decay_down: bfloat16 [2048, 64], replicated, may hold values from -0.125 to 0.125
- decay_up: bfloat16 [64, 1024], replicated, may hold values from -0.75 to 0.75
- decay_bias: float32 [1024], replicated, may hold values from -4 to 1
- rate_down: bfloat16 [2048, 64], replicated, may hold values from -0.125 to 0.125
- rate_up: bfloat16 [64, 1024], replicated, may hold values from -0.75 to 0.75
- rate_bias: float32 [1024], replicated, may hold values from -4 to 4
- head_gain: float32 [1024], replicated, may hold values from 0.1 to 1.9
- out_weight: bfloat16 [1024, 2048], P('tp'), may hold values from -0.1875 to 0.1875
- memory_state: float32 [1024, 16, 64, 64], P('ep', 'tp'), may hold values from -6 to 6
- ffn_gain: float32 [2048], replicated, may hold values from 0.1 to 1.9
- blend_vector: bfloat16 [2048], replicated, may hold values from -0.125 to 0.125
- dense_gate: bfloat16 [2048, 5632], P(None, ('ep', 'tp')), may hold values from -0.125 to 0.125
- dense_up: bfloat16 [2048, 5632], P(None, ('ep', 'tp')), may hold values from -0.125 to 0.125
- dense_down: bfloat16 [5632, 2048], P(('ep', 'tp')), may hold values from -0.3125 to 0.3125
- expert_gate: bfloat16 [16, 2048, 1536], P('ep', None, 'tp'), may hold values from -0.125 to 0.125
- expert_up: bfloat16 [16, 2048, 1536], P('ep', None, 'tp'), may hold values from -0.125 to 0.125
- expert_down: bfloat16 [16, 1536, 2048], P('ep', 'tp'), may hold values from -0.15625 to 0.15625
- routing: int32 [1024, 2], P('ep'), may hold values from 0 to 15, all different within a row; in each aligned block of 64 rows (0 to 63, 64 to 127, ...) at most 16 rows name the same one
- route_scale: float32 [1024, 2], P('ep'), may hold values from 0.25 to 1
Outputs:
- layer_out: bfloat16 [1024, 2048], P('ep')
- new_state: float32 [1024, 16, 64, 64], P('ep', 'tp')
Inputs may be any that keep to these rules, and one draw needn't show every extreme that they name: `routing`: among the 64 sequences of one index of ep, no expert is chosen more than 16 times, and some expert is chosen exactly 16 times; a sequence's 2 choices differ.
All inputs are finite; a program needn't handle non-finite values.
Results may differ from a plain program's by a relative error of at most 0.017.
Values may be sent and summed in bfloat16 or wider, within the bound.
No kernel may reach another device: no remote copies, remote signals or barrier semaphores. Data moves between devices by JAX's collectives and lax.ppermute only.
A program may use at most 192 MiB of HBM per device.

v0:
```python
import jax
import jax.numpy as jnp
from jax import lax
from jax.sharding import PartitionSpec as P


def stored(tensor):
    return lax.optimization_barrier(tensor.astype(jnp.bfloat16)).astype(jnp.float32)


def rms_scaled(tensor, gain_vec):
    values = tensor.astype(jnp.float32)
    return values * lax.rsqrt(jnp.mean(values * values, axis=-1, keepdims=True) + 1e-06) * gain_vec


def silu_of(tensor):
    return tensor / (1.0 + jnp.exp(-tensor))


def matmul(left, right):
    return jnp.dot(left, right, preferred_element_type=jnp.float32)


def shards(
    hidden,
    mix_gain,
    recept_weight,
    key_weight,
    value_weight,
    decay_down,
    decay_up,
    decay_bias,
    rate_down,
    rate_up,
    rate_bias,
    head_gain,
    out_weight,
    memory_state,
    ffn_gain,
    blend_vector,
    dense_gate,
    dense_up,
    dense_down,
    expert_gate,
    expert_up,
    expert_down,
    routing,
    route_scale,
):
    seq_count, model_width = hidden.shape
    own_width = recept_weight.shape[1]
    head_count = memory_state.shape[1]
    head_size = memory_state.shape[2]
    offset = lax.axis_index("tp") * own_width
    decay_up_own = lax.dynamic_slice_in_dim(decay_up, offset, own_width, 1)
    rate_up_own = lax.dynamic_slice_in_dim(rate_up, offset, own_width, 1)
    decay_bias_own = lax.dynamic_slice_in_dim(decay_bias, offset, own_width, 0)
    rate_bias_own = lax.dynamic_slice_in_dim(rate_bias, offset, own_width, 0)
    gain_own = lax.dynamic_slice_in_dim(head_gain, offset, own_width, 0)
    normed_in = rms_scaled(hidden, mix_gain).astype(jnp.bfloat16)
    split_shape = (seq_count, head_count, head_size)
    recept_rows = stored(matmul(normed_in, recept_weight)).reshape(split_shape)
    key_rows = stored(matmul(normed_in, key_weight)).reshape(split_shape)
    value_rows = stored(matmul(normed_in, value_weight)).reshape(split_shape)
    decay_low = jnp.tanh(matmul(normed_in, decay_down)).astype(jnp.bfloat16)
    decay_pre = matmul(decay_low, decay_up_own) + decay_bias_own
    decay_rate = jnp.exp(-jnp.exp(-jax.nn.softplus(-decay_pre) - 0.5)).reshape(split_shape)
    rate_low = matmul(normed_in, rate_down).astype(jnp.bfloat16)
    learn_rate = jax.nn.sigmoid(matmul(rate_low, rate_up_own) + rate_bias_own).reshape(split_shape)
    unit_key = key_rows * lax.rsqrt(jnp.sum(key_rows * key_rows, axis=-1, keepdims=True) + 1e-06)
    removed = jnp.einsum("shij,shj->shi", memory_state, unit_key, precision=lax.Precision.HIGHEST)
    new_state = (
        memory_state * decay_rate[:, :, None, :]
        - removed[..., None] * (unit_key * learn_rate)[:, :, None, :]
        + value_rows[..., None] * (key_rows * learn_rate)[:, :, None, :]
    )
    readout = jnp.einsum("shij,shj->shi", new_state, recept_rows, precision=lax.Precision.HIGHEST)
    centre = jnp.mean(readout, axis=-1, keepdims=True)
    variance = jnp.mean(jnp.square(readout - centre), axis=-1, keepdims=True)
    head_normed = (
        (
            (readout - centre)
            * lax.rsqrt(variance + 0.00064)
            * gain_own.reshape(head_count, head_size)
        )
        .astype(jnp.bfloat16)
        .reshape(seq_count, own_width)
    )
    attn_sum = lax.psum(matmul(head_normed, out_weight).astype(jnp.bfloat16), "tp").astype(
        jnp.float32
    )
    first_res = (hidden.astype(jnp.float32) + attn_sum).astype(jnp.bfloat16)
    ffn_in = rms_scaled(first_res, ffn_gain).astype(jnp.bfloat16)
    blend = jax.nn.sigmoid(jnp.dot(ffn_in, blend_vector, preferred_element_type=jnp.float32))
    piece = lax.all_gather(ffn_in, "ep", axis=0, tiled=True)
    dense_act = (silu_of(matmul(piece, dense_gate)) * matmul(piece, dense_up)).astype(jnp.bfloat16)
    own_units = lax.all_to_all(dense_act, "ep", split_axis=0, concat_axis=1, tiled=True)
    dense_out = matmul(own_units, lax.all_gather(dense_down, "ep", axis=0, tiled=True))
    dest_count = lax.axis_size("ep")
    top_count = routing.shape[1]
    slot_cap = max(2, 2 * seq_count * top_count // dest_count)
    flat_route = routing.reshape(-1)
    one_hot = (flat_route[:, None] == jnp.arange(dest_count, dtype=jnp.int32)[None, :]).astype(
        jnp.int32
    )
    running = jnp.cumsum(one_hot, axis=0)
    rank = jnp.sum((running - 1) * one_hot, axis=1)
    slot = flat_route * slot_cap + rank
    select = (slot[None, :] == jnp.arange(dest_count * slot_cap, dtype=jnp.int32)[:, None]).astype(
        jnp.bfloat16
    )
    pair_rows = jnp.repeat(ffn_in, top_count, axis=0)
    outgoing = (
        matmul(select, pair_rows).astype(jnp.bfloat16).reshape(dest_count, slot_cap, model_width)
    )
    arrived = lax.all_to_all(outgoing, "ep", split_axis=0, concat_axis=0, tiled=True)
    src_count, slot_items, width_in = arrived.shape
    flat_in = arrived.reshape(src_count * slot_items, width_in)
    expert_act = (silu_of(matmul(flat_in, expert_gate[0])) * matmul(flat_in, expert_up[0])).astype(
        jnp.bfloat16
    )
    result = matmul(expert_act, expert_down[0]).reshape(src_count, slot_items, width_in)
    returned = lax.all_to_all(
        result.astype(jnp.bfloat16), "ep", split_axis=0, concat_axis=0, tiled=True
    ).astype(result.dtype)
    per_pair = jnp.take(returned.reshape(dest_count * slot_cap, model_width), slot, axis=0)
    expert_sum = jnp.sum(
        per_pair.reshape(seq_count, top_count, model_width) * route_scale[:, :, None], axis=1
    )
    mixed = lax.psum((expert_sum + blend[:, None] * dense_out).astype(jnp.bfloat16), "tp").astype(
        jnp.float32
    )
    layer_out = (first_res.astype(jnp.float32) + mixed).astype(jnp.bfloat16)
    return (layer_out, new_state)


def solution(mesh):
    in_specs = (
        P("ep", None),
        P(),
        P(None, "tp"),
        P(None, "tp"),
        P(None, "tp"),
        P(),
        P(),
        P(),
        P(),
        P(),
        P(),
        P(),
        P("tp", None),
        P("ep", "tp", None, None),
        P(),
        P(),
        P(None, ("ep", "tp")),
        P(None, ("ep", "tp")),
        P(("ep", "tp"), None),
        P("ep", None, "tp"),
        P("ep", None, "tp"),
        P("ep", "tp", None),
        P("ep", None),
        P("ep", None),
    )
    out_specs = (P("ep", None), P("ep", "tp", None, None))
    return jax.shard_map(shards, mesh=mesh, in_specs=in_specs, out_specs=out_specs, check_vma=False)
```

profile of v0, /device:TPU:0, one launch (start us, length us, event | category | flops | bytes accessed | tf_op | source)
XLA Modules:
  0.0 408.8 jit_solution(1007329135840309137)
XLA Ops:
  9.3 1.5 fusion.21
  11.6 2.2 convolution_convert_fusion.4
  19.4 2.1 convolution_convert_fusion.3
  22.3 2.1 convolution_convert_fusion.2
  26.7 29.5 %fusion.56 = f32[64,8,1,64]{3,2,1,0:T(1,128)S(1)} fusion(f32[64,8,64,1]{2,3,1,0:T(1,128)S(1)} %bitcast.78, f32[64,8,64,64]{3,2,1,0:T(8,128)} %param.37), kind=kOutput, calls=%fused_computation.85 | convolution fusion | flops 25165824 | bytes 8650752 | tf_op jit(solution)/shard_map/shij,shj->shi/dot_general | solution.py:71
  56.3 11.9 %multiply_add_fusion = f32[64,8,64,64]{3,2,1,0:T(8,128)} fusion(f32[64,8,64,64]{3,2,1,0:T(8,128)S(1)} %bitcast.71, f32[64,8,64]{2,1,0:T(8,128)S(1)} %get-tuple-element.4, f32[64,8,64]{2,1,0:T(8,128)S(1)} %copy-done.3, f32[64,8,64]{2,1,0:T(8,128)S(1)} %get-tuple-element.2, f32[64,8,64]{2,1,0:T(8,128)S(1)} %bitcast.77, f32[64,8,64]{2,1,0:T(8,128)S(1)} %copy-done.4), kind=kLoop, calls=%fused_computation.1 | loop fusion | flops 10485760 | bytes 17432576 | tf_op jit(solution)/shard_map/add | solution.py:73
  68.2 16.3 %fusion.57 = f32[64,8,1,64]{3,2,1,0:T(1,128)} fusion(f32[64,8,64,64]{3,2,1,0:T(8,128)} %multiply_add_fusion, bf16[64,8,64,1]{2,3,1,0:T(2,128)(2,1)S(1)} %copy-done.2), kind=kOutput, calls=%fused_computation.86 | convolution fusion | flops 25165824 | bytes 8585216 | tf_op jit(solution)/shard_map/shij,shj->shi/dot_general | solution.py:77
  90.2 2.8 convolution_convert_fusion.1
  93.3 20.9 %all-reduce.3.cloned.1.call-done = bf16[64,2048]{1,0:T(8,128)(2,1)} async-done(((bf16[64,2048]{1,0:T(8,128)(2,1)}), bf16[64,2048]{1,0:T(8,128)(2,1)}) %all-reduce.3.cloned.1.call-update) | async-done | bytes 262160 | tf_op jit(solution)/shard_map/psum | solution.py:89
  115.3 1.8 fusion.34
  118.5 2.1 broadcast_in_dim.10
  120.6 2.1 reshape.162
  122.7 1.6 convolution_convert_fusion
  124.3 45.4 %all_to_all.29 = bf16[16,16,2048]{2,1,0:T(8,128)(2,1)S(1)} all-to-all(bf16[16,16,2048]{2,1,0:T(8,128)(2,1)S(1)} %bitcast.75), channel_id=1, replica_groups=mesh['ep'=16,'tp'=2] {'ep'}, dimensions={0} | all-to-all | bytes 2097152 | tf_op jit(solution)/shard_map/all_to_all | solution.py:116
  172.6 2.0 fusion.6
  174.6 6.8 %all-to-all-start.1 = ((bf16[16,16,2048]{2,1,0:T(8,128)(2,1)}), bf16[16,16,2048]{2,1,0:T(8,128)(2,1)}, u32[]{:S(2)}, u32[]{:S(2)}) async-start(bf16[16,16,2048]{2,1,0:T(8,128)(2,1)} %fusion.6), calls=%async_computation.1 | async-start | bytes 2097152 | tf_op jit(solution)/shard_map/all_to_all | solution.py:123
  183.3 38.9 %all-gather.3.cloned.1.call-done = bf16[1024,2048]{1,0:T(8,128)(2,1)} async-done(((bf16[64,2048]{1,0:T(8,128)(2,1)}), bf16[1024,2048]{1,0:T(8,128)(2,1)}) %all-gather.3.cloned.1.call-update) | async-done | bytes 4194320 | tf_op jit(solution)/shard_map/all_gather | solution.py:95
  222.2 4.1 fusion.58
  226.3 2.3 fusion.17
  228.6 2.0 copy.44
  230.6 4.7 %all-to-all-start.2 = ((bf16[16,64,176]{2,1,0:T(8,128)(2,1)}), bf16[16,64,176]{2,1,0:T(8,128)(2,1)}, u32[]{:S(2)}, u32[]{:S(2)}) async-start(bf16[16,64,176]{2,1,0:T(8,128)(2,1)} %bitcast.76), calls=%async_computation.2 | async-start | bytes 1048576 | tf_op jit(solution)/shard_map/all_to_all | solution.py:97
  235.6 2.9 bitcast_convert_fusion
  238.5 4.0 gather_fusion
  242.5 2.8 gather.7
  245.3 4.2 %multiply_reduce_fusion = f32[64,2048]{1,0:T(8,128)} fusion(f32[64,2,2048]{2,1,0:T(2,128)} %gather.7, pred[64,2]{1,0:T(8,128)(4,1)S(1)} %copy.41, f32[64,2]{1,0:T(8,128)S(1)} %copy.43), kind=kLoop, calls=%fused_computation.37 | loop fusion | flops 655360 | bytes 1573504 | tf_op jit(solution)/shard_map/reduce_sum | solution.py:127
  249.5 8.7 %all-to-all-done.2 = bf16[16,64,176]{2,1,0:T(8,128)(2,1)} async-done(((bf16[16,64,176]{2,1,0:T(8,128)(2,1)}), bf16[16,64,176]{2,1,0:T(8,128)(2,1)}, u32[]{:S(2)}, u32[]{:S(2)}) %all-to-all-start.2) | async-done | bytes 360480 | tf_op jit(solution)/shard_map/all_to_all | solution.py:97
  258.2 2.1 copy.45
  260.3 2.5 all_to_all.25
  262.8 113.8 %all-gather.5.cloned.1.call-done = bf16[2816,2048]{1,0:T(8,128)(2,1)} async-done(((bf16[176,2048]{1,0:T(8,128)(2,1)}), bf16[2816,2048]{1,0:T(8,128)(2,1)}) %all-gather.5.cloned.1.call-update) | async-done | bytes 11534352 | tf_op jit(solution)/shard_map/all_gather | solution.py:98
  376.6 7.2 %fusion.10 = bf16[64,2048]{1,0:T(8,128)(2,1)} fusion(f32[64,2048]{1,0:T(8,128)} %multiply_reduce_fusion, bf16[64,2816]{1,0:T(8,128)(2,1)} %all_to_all.25, bf16[2816,2048]{1,0:T(8,128)(2,1)} %all-gather.5.cloned.1.call-done, f32[64]{0:T(128)S(1)} %fusion.27), kind=kOutput, calls=%fused_computation.13 | convolution fusion | flops 738590720 | bytes 12681472 | tf_op jit(solution)/shard_map/dot_general | solution.py:21
  383.9 16.6 %all-reduce.5.cloned.1.call-done = bf16[64,2048]{1,0:T(8,128)(2,1)} async-done(((bf16[64,2048]{1,0:T(8,128)(2,1)}), bf16[64,2048]{1,0:T(8,128)(2,1)}) %all-reduce.5.cloned.1.call-update) | async-done | bytes 262160 | tf_op jit(solution)/shard_map/psum | solution.py:130
  400.4 1.8 fusion.35
  (95 shorter events, 24.9 us)
Async XLA Ops:
  7.2 165.4 %copy-start = (bf16[1,768,2048]{2,1,0:T(8,128)(2,1)S(1)}, bf16[1,768,2048]{2,1,0:T(8,128)(2,1)}, u32[]{:S(2)}) copy-start(bf16[1,768,2048]{2,1,0:T(8,128)(2,1)} %param.45) | copy-start | bytes 9437188
  7.2 9.9 %copy-start.1 = (bf16[64,2048]{1,0:T(8,128)(2,1)S(1)}, bf16[64,2048]{1,0:T(8,128)(2,1)}, u32[]{:S(2)}) copy-start(bf16[64,2048]{1,0:T(8,128)(2,1)} %param.24) | copy-start | bytes 786436
  7.2 9.9 %copy-start.7 = (f32[2048]{0:T(1024)S(1)}, f32[2048]{0:T(1024)}, u32[]{:S(2)}) copy-start(f32[2048]{0:T(1024)} %param.25) | copy-start | bytes 24580
  7.2 106.9 %all-reduce.3.cloned.1.call-start = ((), (), s32[]{:S(2)}) async-start(), calls=%async_computation.3 | async-start | bytes 524288 | tf_op jit(solution)/shard_map/psum | solution.py:89
  19.4 5.9 %copy-start.6 = (f32[64,8]{1,0:T(8,128)S(1)}, f32[64,8]{1,0:T(8,128)}, u32[]{:S(2)}) copy-start(f32[64,8]{1,0:T(8,128)} %add_rsqrt_fusion.1) | copy-start | bytes 6148
  25.3 30.9 %slice-start = ((s8[16777216]{0:T(1024)(128)(4,1)}), s8[4194304]{0:T(1024)(128)(4,1)S(1)}, s32[]{:S(2)}) async-start(s8[16777216]{0:T(1024)(128)(4,1)} %bitcast.70), calls=%async_computation.7 | async-start | bytes 8388608
  26.7 29.6 %slice-start.1 = ((s8[16777216]{0:T(1024)(128)(4,1)}), s8[4194304]{0:T(1024)(128)(4,1)S(1)}, s32[]{:S(2)}) async-start(s8[16777216]{0:T(1024)(128)(4,1)} %bitcast.70), calls=%async_computation.8 | async-start | bytes 8388608
  26.7 29.6 %slice-start.2 = ((s8[16777216]{0:T(1024)(128)(4,1)}), s8[4194304]{0:T(1024)(128)(4,1)S(1)}, s32[]{:S(2)}) async-start(s8[16777216]{0:T(1024)(128)(4,1)} %bitcast.70), calls=%async_computation.9 | async-start | bytes 8388608
  26.7 29.6 %slice-start.3 = ((s8[16777216]{0:T(1024)(128)(4,1)}), s8[4194304]{0:T(1024)(128)(4,1)S(1)}, s32[]{:S(2)}) async-start(s8[16777216]{0:T(1024)(128)(4,1)} %bitcast.70), calls=%async_computation.10 | async-start | bytes 8388608
  26.7 29.6 %copy-start.3 = (f32[64,8,64]{2,1,0:T(8,128)S(1)}, f32[64,8,64]{2,1,0:T(8,128)}, u32[]{:S(2)}) copy-start(f32[64,8,64]{2,1,0:T(8,128)} %reshape.169) | copy-start | bytes 393220
  26.7 29.6 %copy-start.4 = (f32[64,8,64]{2,1,0:T(8,128)S(1)}, f32[64,8,64]{2,1,0:T(8,128)}, u32[]{:S(2)}) copy-start(f32[64,8,64]{2,1,0:T(8,128)} %mul.187) | copy-start | bytes 393220
  56.3 11.9 %copy-start.2 = (bf16[64,8,64,1]{2,3,1,0:T(2,128)(2,1)S(1)}, bf16[64,8,64,1]{2,3,1,0:T(2,128)(2,1)}, u32[]{:S(2)}) copy-start(bf16[64,8,64,1]{2,3,1,0:T(2,128)(2,1)} %reshape.188) | copy-start | bytes 196612
  68.2 19.9 %copy-start.12 = (f32[1024]{0:T(1024)S(1)}, f32[1024]{0:T(1024)}, u32[]{:S(2)}) copy-start(f32[1024]{0:T(1024)} %param.35) | copy-start | bytes 12292
  84.5 30.8 %copy-start.9 = (f32[2048]{0:T(1024)S(1)}, f32[2048]{0:T(1024)}, u32[]{:S(2)}) copy-start(f32[2048]{0:T(1024)} %param.38) | copy-start | bytes 24580
  84.5 33.3 %copy-start.8 = (s32[64,2]{0,1:T(2,128)S(1)}, s32[64,2]{0,1:T(2,128)}, u32[]{:S(2)}) copy-start(s32[64,2]{0,1:T(2,128)} %param.46) | copy-start | bytes 1540
  85.7 0.6 copy-start.5
  93.0 129.2 %all-gather.3.cloned.1.call-start = ((), (), s32[]{:S(2)}) async-start(), calls=%async_computation.4 | async-start | bytes 4456448 | tf_op jit(solution)/shard_map/all_gather | solution.py:95
  117.1 259.5 %all-gather.5.cloned.1.call-start = ((), (), s32[]{:S(2)}) async-start(), calls=%async_computation.5 | async-start | bytes 12255232 | tf_op jit(solution)/shard_map/all_gather | solution.py:98
  122.7 47.0 %copy-start.14 = (bf16[1,2048,768]{2,1,0:T(8,128)(2,1)S(1)}, bf16[1,2048,768]{2,1,0:T(8,128)(2,1)}, u32[]{:S(2)}) copy-start(bf16[1,2048,768]{2,1,0:T(8,128)(2,1)} %param.43) | copy-start | bytes 9437188
  169.7 1.9 copy-start.15
  172.6 9.4 %copy-start.11 = (f32[64,2]{0,1:T(2,128)S(1)}, f32[64,2]{0,1:T(2,128)}, u32[]{:S(2)}) copy-start(f32[64,2]{0,1:T(2,128)} %param.47) | copy-start | bytes 1540
  172.6 9.5 %copy-start.10 = (bf16[2048]{0:T(1024)(128)(2,1)S(1)}, bf16[2048]{0:T(1024)(128)(2,1)}, u32[]{:S(2)}) copy-start(bf16[2048]{0:T(1024)(128)(2,1)} %param.39) | copy-start | bytes 12292
  174.6 56.0 %all-to-all-start.1 = ((bf16[16,16,2048]{2,1,0:T(8,128)(2,1)}), bf16[16,16,2048]{2,1,0:T(8,128)(2,1)}, u32[]{:S(2)}, u32[]{:S(2)}) async-start(bf16[16,16,2048]{2,1,0:T(8,128)(2,1)} %fusion.6), calls=%async_computation.1 | async-start | bytes 2097152 | tf_op jit(solution)/shard_map/all_to_all | solution.py:123
  222.2 4.1 copy-start.13
  222.2 4.1 copy-start.16
  230.6 27.6 %all-to-all-start.2 = ((bf16[16,64,176]{2,1,0:T(8,128)(2,1)}), bf16[16,64,176]{2,1,0:T(8,128)(2,1)}, u32[]{:S(2)}, u32[]{:S(2)}) async-start(bf16[16,64,176]{2,1,0:T(8,128)(2,1)} %bitcast.76), calls=%async_computation.2 | async-start | bytes 1048576 | tf_op jit(solution)/shard_map/all_to_all | solution.py:97
  235.3 165.1 %all-reduce.5.cloned.1.call-start = ((), (), s32[]{:S(2)}) async-start(), calls=%async_computation.6 | async-start | bytes 524288 | tf_op jit(solution)/shard_map/psum | solution.py:130
Sparse Core Ops, SparseCore 0:
  93.1 20.9 all-reduce.2
  117.5 104.6 all-gather.2
  224.9 151.6 all-gather.4
  384.0 16.3 all-reduce.4
where the time goes:
time: 410 us; the launch traced here: 409 us
  waiting for transfers between devices  200 us (49%)
  matrix products  78.4 us (19%)
  blocking collectives  45.4 us (11%)
  other arithmetic  32.6 us (8%)
  local copies, waits for them, and re-layouts  26.6 us (6%)
  between operations  14.2 us (3%)
  starting transfers between devices  12.1 us (3%)
    all_gather x1, waiting for transfers between devices, shards(): lax.all_gather(dense_down, 'ep', axis=0, tiled=True)  114 us
    all_to_all x1, blocking collectives, shards(): lax.all_to_all(outgoing, 'ep', split_axis=0, concat_axis=0, tiled=True)  45.4 us
    all_gather x1, waiting for transfers between devices, shards(): piece = lax.all_gather(ffn_in, 'ep', axis=0, tiled=True)  38.9 us
    dot_general x13, matrix products, matmul(): return jnp.dot(left, right, preferred_element_type=jnp.float32)  31.5 us
    dot_general x1, matrix products, shards(): jnp.einsum('shij,shj->shi', memory_state, unit_key, precision=lax.Precisi...  29.5 us
    psum x1, waiting for transfers between devices, shards(): lax.psum(matmul(head_normed, out_weight).astype(jnp.bfloat16), 'tp')  20.9 us
    psum x1, waiting for transfers between devices, shards(): lax.psum((expert_sum + blend[:, None] * dense_out).astype(jnp.bfloat16),...  16.6 us
    dot_general x1, matrix products, shards(): jnp.einsum('shij,shj->shi', new_state, recept_rows, precision=lax.Precisi...  16.3 us
  transfers between devices with their start and end apart: 6, of which 5 were waited for; matrix products, arithmetic and copies ran while one was open for 9% of the time, Pallas kernels for 0%

commit v1 on v0

--- a/solution.py
+++ b/solution.py
@@ -86,9 +86,9 @@
         .astype(jnp.bfloat16)
         .reshape(seq_count, own_width)
     )
-    attn_sum = lax.psum(matmul(head_normed, out_weight).astype(jnp.bfloat16), "tp").astype(
-        jnp.float32
-    )
+    attn_sum = jnp.sum(
+        lax.all_gather(matmul(head_normed, out_weight).astype(jnp.bfloat16), "tp"), axis=0
+    ).astype(jnp.float32)
     first_res = (hidden.astype(jnp.float32) + attn_sum).astype(jnp.bfloat16)
     ffn_in = rms_scaled(first_res, ffn_gain).astype(jnp.bfloat16)
     blend = jax.nn.sigmoid(jnp.dot(ffn_in, blend_vector, preferred_element_type=jnp.float32))

time: 410 us -> 394 us (0.961)
  waiting for transfers between devices: 200 us -> 178 us
    psum x1 -> x0, waiting for transfers between devices: 20.9 us -> none  [shards(): lax.psum(matmul(head_normed, out_weight).astype(jnp.bfloat16), 'tp')]
  transfers between devices with their start and end apart: 6 -> 5, of which waited for: 5 -> 4; matrix products, arithmetic and copies ran while one was open for 9% -> 9% of each run, Pallas kernels for 0% -> 0%
where the time goes in v1:
time: 394 us; the launch traced here: 392 us
  waiting for transfers between devices  178 us (45%)
  matrix products  77.7 us (20%)
  blocking collectives  49.4 us (13%)
  other arithmetic  34.4 us (9%)
  local copies, waits for them, and re-layouts  26.6 us (7%)
  between operations  14.2 us (4%)
  starting transfers between devices  11.7 us (3%)
    all_gather x1, waiting for transfers between devices, shards(): lax.all_gather(dense_down, 'ep', axis=0, tiled=True)  114 us
    all_to_all x1, blocking collectives, shards(): lax.all_to_all(outgoing, 'ep', split_axis=0, concat_axis=0, tiled=True)  46.8 us
    all_gather x1, waiting for transfers between devices, shards(): piece = lax.all_gather(ffn_in, 'ep', axis=0, tiled=True)  38.7 us
    dot_general x13, matrix products, matmul(): return jnp.dot(left, right, preferred_element_type=jnp.float32)  30.7 us
    dot_general x1, matrix products, shards(): jnp.einsum('shij,shj->shi', memory_state, unit_key, precision=lax.Precisi...  29.5 us
    psum x1, waiting for transfers between devices, shards(): lax.psum((expert_sum + blend[:, None] * dense_out).astype(jnp.bfloat16),...  16.6 us
    dot_general x1, matrix products, shards(): jnp.einsum('shij,shj->shi', new_state, recept_rows, precision=lax.Precisi...  16.3 us
    add x1, other arithmetic, shards(): memory_state * decay_rate[:, :, None, :]  11.9 us
  transfers between devices with their start and end apart: 5, of which 4 were waited for; matrix products, arithmetic and copies ran while one was open for 9% of the time, Pallas kernels for 0%

profile of v1, /device:TPU:0, one launch (start us, length us, event | category | flops | bytes accessed | tf_op | source)
XLA Modules:
  0.0 392.4 jit_solution(64338413010126682)
XLA Ops:
  11.6 2.2 convolution_convert_fusion.4
  19.4 2.1 convolution_convert_fusion.3
  22.3 2.1 convolution_convert_fusion.2
  26.7 29.5 %fusion.56 = f32[64,8,1,64]{3,2,1,0:T(1,128)S(1)} fusion(f32[64,8,64,1]{2,3,1,0:T(1,128)S(1)} %bitcast.80, f32[64,8,64,64]{3,2,1,0:T(8,128)} %param.37), kind=kOutput, calls=%fused_computation.85 | convolution fusion | flops 25165824 | bytes 8650752 | tf_op jit(solution)/shard_map/shij,shj->shi/dot_general | solution.py:71
  56.3 11.9 %multiply_add_fusion = f32[64,8,64,64]{3,2,1,0:T(8,128)} fusion(f32[64,8,64,64]{3,2,1,0:T(8,128)S(1)} %bitcast.72, f32[64,8,64]{2,1,0:T(8,128)S(1)} %get-tuple-element.4, f32[64,8,64]{2,1,0:T(8,128)S(1)} %copy-done.3, f32[64,8,64]{2,1,0:T(8,128)S(1)} %get-tuple-element.2, f32[64,8,64]{2,1,0:T(8,128)S(1)} %bitcast.79, f32[64,8,64]{2,1,0:T(8,128)S(1)} %copy-done.4), kind=kLoop, calls=%fused_computation.1 | loop fusion | flops 10485760 | bytes 17432576 | tf_op jit(solution)/shard_map/add | solution.py:73
  68.2 16.3 %fusion.57 = f32[64,8,1,64]{3,2,1,0:T(1,128)} fusion(f32[64,8,64,64]{3,2,1,0:T(8,128)} %multiply_add_fusion, bf16[64,8,64,1]{2,3,1,0:T(2,128)(2,1)S(1)} %copy-done.2), kind=kOutput, calls=%fused_computation.86 | convolution fusion | flops 25165824 | bytes 8585216 | tf_op jit(solution)/shard_map/shij,shj->shi/dot_general | solution.py:77
  90.1 2.1 convolution_convert_fusion.1
  92.3 2.6 all-gather
  94.9 1.9 reduce_sum.83
  97.9 1.8 fusion.34
  100.5 2.1 broadcast_in_dim.10
  102.6 2.0 reshape.162
  105.3 1.6 convolution_convert_fusion
  106.9 46.8 %all_to_all.29 = bf16[16,16,2048]{2,1,0:T(8,128)(2,1)S(1)} all-to-all(bf16[16,16,2048]{2,1,0:T(8,128)(2,1)S(1)} %bitcast.76), channel_id=1, replica_groups=mesh['ep'=16,'tp'=2] {'ep'}, dimensions={0} | all-to-all | bytes 2097152 | tf_op jit(solution)/shard_map/all_to_all | solution.py:116
  156.7 2.0 fusion.6
  158.6 6.6 %all-to-all-start.1 = ((bf16[16,16,2048]{2,1,0:T(8,128)(2,1)}), bf16[16,16,2048]{2,1,0:T(8,128)(2,1)}, u32[]{:S(2)}, u32[]{:S(2)}) async-start(bf16[16,16,2048]{2,1,0:T(8,128)(2,1)} %fusion.6), calls=%async_computation.1 | async-start | bytes 2097152 | tf_op jit(solution)/shard_map/all_to_all | solution.py:123
  167.2 38.7 %all-gather.4.cloned.1.call-done = bf16[1024,2048]{1,0:T(8,128)(2,1)} async-done(((bf16[64,2048]{1,0:T(8,128)(2,1)}), bf16[1024,2048]{1,0:T(8,128)(2,1)}) %all-gather.4.cloned.1.call-update) | async-done | bytes 4194320 | tf_op jit(solution)/shard_map/all_gather | solution.py:95
  205.8 4.1 %fusion.58 = f32[1024,176]{0,1:T(8,128)S(1)} fusion(bf16[1024,2048]{1,0:T(8,128)(2,1)} %all-gather.4.cloned.1.call-done, bf16[2048,176]{0,1:T(8,128)(2,1)} %param.40), kind=kOutput, calls=%fused_computation.87 | convolution fusion | flops 738197504 | bytes 5636096 | tf_op jit(solution)/shard_map/dot_general | solution.py:21
  209.9 2.3 fusion.17
  212.2 2.0 copy.44
  214.2 4.7 %all-to-all-start.2 = ((bf16[16,64,176]{2,1,0:T(8,128)(2,1)}), bf16[16,64,176]{2,1,0:T(8,128)(2,1)}, u32[]{:S(2)}, u32[]{:S(2)}) async-start(bf16[16,64,176]{2,1,0:T(8,128)(2,1)} %bitcast.77), calls=%async_computation.2 | async-start | bytes 1048576 | tf_op jit(solution)/shard_map/all_to_all | solution.py:97
  219.2 2.9 bitcast_convert_fusion
  222.1 4.0 %gather_fusion = f32[128,2048]{1,0:T(8,128)} fusion(f32[256,2048]{1,0:T(8,128)} %bitcast_convert_fusion, s32[1024]{0:T(1024)S(1)} %pad_clamp_fusion), kind=kCustom, calls=%fused_computation | custom fusion | bytes 2097664 | tf_op jit(solution)/shard_map/jit(_take)/gather | solution.py:126
  226.1 2.8 gather.7
  229.0 4.2 %multiply_reduce_fusion = f32[64,2048]{1,0:T(8,128)} fusion(f32[64,2,2048]{2,1,0:T(2,128)} %gather.7, pred[64,2]{1,0:T(8,128)(4,1)S(1)} %copy.41, f32[64,2]{1,0:T(8,128)S(1)} %copy.43), kind=kLoop, calls=%fused_computation.37 | loop fusion | flops 655360 | bytes 1573504 | tf_op jit(solution)/shard_map/reduce_sum | solution.py:127
  233.1 8.7 %all-to-all-done.2 = bf16[16,64,176]{2,1,0:T(8,128)(2,1)} async-done(((bf16[16,64,176]{2,1,0:T(8,128)(2,1)}), bf16[16,64,176]{2,1,0:T(8,128)(2,1)}, u32[]{:S(2)}, u32[]{:S(2)}) %all-to-all-start.2) | async-done | bytes 360480 | tf_op jit(solution)/shard_map/all_to_all | solution.py:97
  241.9 2.1 copy.45
  244.0 2.5 all_to_all.25
  246.5 113.7 %all-gather.6.cloned.1.call-done = bf16[2816,2048]{1,0:T(8,128)(2,1)} async-done(((bf16[176,2048]{1,0:T(8,128)(2,1)}), bf16[2816,2048]{1,0:T(8,128)(2,1)}) %all-gather.6.cloned.1.call-update) | async-done | bytes 11534352 | tf_op jit(solution)/shard_map/all_gather | solution.py:98
  360.2 7.2 %fusion.10 = bf16[64,2048]{1,0:T(8,128)(2,1)} fusion(f32[64,2048]{1,0:T(8,128)} %multiply_reduce_fusion, bf16[64,2816]{1,0:T(8,128)(2,1)} %all_to_all.25, bf16[2816,2048]{1,0:T(8,128)(2,1)} %all-gather.6.cloned.1.call-done, f32[64]{0:T(128)S(1)} %fusion.27), kind=kOutput, calls=%fused_computation.13 | convolution fusion | flops 738590720 | bytes 12681472 | tf_op jit(solution)/shard_map/dot_general | solution.py:21
  367.5 16.6 %all-reduce.2.cloned.1.call-done = bf16[64,2048]{1,0:T(8,128)(2,1)} async-done(((bf16[64,2048]{1,0:T(8,128)(2,1)}), bf16[64,2048]{1,0:T(8,128)(2,1)}) %all-reduce.2.cloned.1.call-update) | async-done | bytes 262160 | tf_op jit(solution)/shard_map/psum | solution.py:130
  384.1 1.8 fusion.35
  (94 shorter events, 26.1 us)
Async XLA Ops:
  7.2 149.5 %copy-start = (bf16[1,768,2048]{2,1,0:T(8,128)(2,1)S(1)}, bf16[1,768,2048]{2,1,0:T(8,128)(2,1)}, u32[]{:S(2)}) copy-start(bf16[1,768,2048]{2,1,0:T(8,128)(2,1)} %param.45) | copy-start | bytes 9437188
  7.2 9.9 %copy-start.1 = (bf16[64,2048]{1,0:T(8,128)(2,1)S(1)}, bf16[64,2048]{1,0:T(8,128)(2,1)}, u32[]{:S(2)}) copy-start(bf16[64,2048]{1,0:T(8,128)(2,1)} %param.24) | copy-start | bytes 786436
  7.2 9.9 %copy-start.7 = (f32[2048]{0:T(1024)S(1)}, f32[2048]{0:T(1024)}, u32[]{:S(2)}) copy-start(f32[2048]{0:T(1024)} %param.25) | copy-start | bytes 24580
  7.2 198.6 %all-gather.4.cloned.1.call-start = ((), (), s32[]{:S(2)}) async-start(), calls=%async_computation.3 | async-start | bytes 4456448 | tf_op jit(solution)/shard_map/all_gather | solution.py:95
  19.4 5.9 %copy-start.6 = (f32[64,8]{1,0:T(8,128)S(1)}, f32[64,8]{1,0:T(8,128)}, u32[]{:S(2)}) copy-start(f32[64,8]{1,0:T(8,128)} %add_rsqrt_fusion.1) | copy-start | bytes 6148
  25.3 30.9 %slice-start = ((s8[16777216]{0:T(1024)(128)(4,1)}), s8[4194304]{0:T(1024)(128)(4,1)S(1)}, s32[]{:S(2)}) async-start(s8[16777216]{0:T(1024)(128)(4,1)} %bitcast.71), calls=%async_computation.6 | async-start | bytes 8388608
  26.6 29.6 %slice-start.1 = ((s8[16777216]{0:T(1024)(128)(4,1)}), s8[4194304]{0:T(1024)(128)(4,1)S(1)}, s32[]{:S(2)}) async-start(s8[16777216]{0:T(1024)(128)(4,1)} %bitcast.71), calls=%async_computation.7 | async-start | bytes 8388608
  26.6 29.6 %slice-start.2 = ((s8[16777216]{0:T(1024)(128)(4,1)}), s8[4194304]{0:T(1024)(128)(4,1)S(1)}, s32[]{:S(2)}) async-start(s8[16777216]{0:T(1024)(128)(4,1)} %bitcast.71), calls=%async_computation.8 | async-start | bytes 8388608
  26.7 29.6 %slice-start.3 = ((s8[16777216]{0:T(1024)(128)(4,1)}), s8[4194304]{0:T(1024)(128)(4,1)S(1)}, s32[]{:S(2)}) async-start(s8[16777216]{0:T(1024)(128)(4,1)} %bitcast.71), calls=%async_computation.9 | async-start | bytes 8388608
  26.7 29.6 %copy-start.3 = (f32[64,8,64]{2,1,0:T(8,128)S(1)}, f32[64,8,64]{2,1,0:T(8,128)}, u32[]{:S(2)}) copy-start(f32[64,8,64]{2,1,0:T(8,128)} %reshape.169) | copy-start | bytes 393220
  26.7 29.6 %copy-start.4 = (f32[64,8,64]{2,1,0:T(8,128)S(1)}, f32[64,8,64]{2,1,0:T(8,128)}, u32[]{:S(2)}) copy-start(f32[64,8,64]{2,1,0:T(8,128)} %mul.187) | copy-start | bytes 393220
  56.3 11.9 %copy-start.2 = (bf16[64,8,64,1]{2,3,1,0:T(2,128)(2,1)S(1)}, bf16[64,8,64,1]{2,3,1,0:T(2,128)(2,1)}, u32[]{:S(2)}) copy-start(bf16[64,8,64,1]{2,3,1,0:T(2,128)(2,1)} %reshape.189) | copy-start | bytes 196612
  68.2 19.8 %copy-start.12 = (f32[1024]{0:T(1024)S(1)}, f32[1024]{0:T(1024)}, u32[]{:S(2)}) copy-start(f32[1024]{0:T(1024)} %param.35) | copy-start | bytes 12292
  84.5 13.4 %copy-start.9 = (f32[2048]{0:T(1024)S(1)}, f32[2048]{0:T(1024)}, u32[]{:S(2)}) copy-start(f32[2048]{0:T(1024)} %param.38) | copy-start | bytes 24580
  85.6 0.6 copy-start.5
  92.2 12.4 %copy-start.8 = (s32[64,2]{0,1:T(2,128)S(1)}, s32[64,2]{0,1:T(2,128)}, u32[]{:S(2)}) copy-start(s32[64,2]{0,1:T(2,128)} %param.46) | copy-start | bytes 1540
  99.7 260.5 %all-gather.6.cloned.1.call-start = ((), (), s32[]{:S(2)}) async-start(), calls=%async_computation.4 | async-start | bytes 12255232 | tf_op jit(solution)/shard_map/all_gather | solution.py:98
  105.1 48.6 %copy-start.14 = (bf16[1,2048,768]{2,1,0:T(8,128)(2,1)S(1)}, bf16[1,2048,768]{2,1,0:T(8,128)(2,1)}, u32[]{:S(2)}) copy-start(bf16[1,2048,768]{2,1,0:T(8,128)(2,1)} %param.43) | copy-start | bytes 9437188
  153.7 1.9 copy-start.15
  156.6 9.2 %copy-start.11 = (f32[64,2]{0,1:T(2,128)S(1)}, f32[64,2]{0,1:T(2,128)}, u32[]{:S(2)}) copy-start(f32[64,2]{0,1:T(2,128)} %param.47) | copy-start | bytes 1540
  156.7 9.3 %copy-start.10 = (bf16[2048]{0:T(1024)(128)(2,1)S(1)}, bf16[2048]{0:T(1024)(128)(2,1)}, u32[]{:S(2)}) copy-start(bf16[2048]{0:T(1024)(128)(2,1)} %param.39) | copy-start | bytes 12292
  158.6 55.6 %all-to-all-start.1 = ((bf16[16,16,2048]{2,1,0:T(8,128)(2,1)}), bf16[16,16,2048]{2,1,0:T(8,128)(2,1)}, u32[]{:S(2)}, u32[]{:S(2)}) async-start(bf16[16,16,2048]{2,1,0:T(8,128)(2,1)} %fusion.6), calls=%async_computation.1 | async-start | bytes 2097152 | tf_op jit(solution)/shard_map/all_to_all | solution.py:123
  205.8 4.1 %copy-start.13 = (bf16[1024,2048]{1,0:T(8,128)(2,1)S(1)}, bf16[1024,2048]{1,0:T(8,128)(2,1)}, u32[]{:S(2)}) copy-start(bf16[1024,2048]{1,0:T(8,128)(2,1)} %all-gather.4.cloned.1.call-done) | copy-start | bytes 12582916
  205.8 4.1 %copy-start.16 = (bf16[2048,176]{0,1:T(8,128)(2,1)S(1)}, bf16[2048,176]{0,1:T(8,128)(2,1)}, u32[]{:S(2)}) copy-start(bf16[2048,176]{0,1:T(8,128)(2,1)} %param.41) | copy-start | bytes 2162692
  214.2 27.6 %all-to-all-start.2 = ((bf16[16,64,176]{2,1,0:T(8,128)(2,1)}), bf16[16,64,176]{2,1,0:T(8,128)(2,1)}, u32[]{:S(2)}, u32[]{:S(2)}) async-start(bf16[16,64,176]{2,1,0:T(8,128)(2,1)} %bitcast.77), calls=%async_computation.2 | async-start | bytes 1048576 | tf_op jit(solution)/shard_map/all_to_all | solution.py:97
  219.0 165.1 %all-reduce.2.cloned.1.call-start = ((), (), s32[]{:S(2)}) async-start(), calls=%async_computation.5 | async-start | bytes 524288 | tf_op jit(solution)/shard_map/psum | solution.py:130
Sparse Core Ops, SparseCore 0:
  99.8 105.9 all-gather.3
  208.6 151.6 all-gather.5
  367.6 16.3 all-reduce.1
